TPU v7x, 32 devices: a whole 2x2x4 slice. The times are simulated.
32 devices in a mesh: kv: 8 (over z, y), tp: 4 (over x, core).
Axes of the slice: x: 2, y: 2, z: 4, core: 2. Of those that a mesh axis runs over, the one named last changes fastest.
Arguments:
- tokens: bfloat16 [128, 4, 4096], P(None, None, ('kv', 'tp')), may hold values from -6 to 6
- input_norm_gain: float32 [4096], replicated, may hold values from 0.1 to 1.9
- w_query: bfloat16 [4096, 4096], P(None, 'kv'), may hold values from -0.09375 to 0.09375
- w_forget: bfloat16 [4096, 4096], P(None, 'kv'), may hold values from -0.09375 to 0.09375
- w_input: bfloat16 [32, 128, 4096], P('kv', 'tp'), may hold values from -0.09375 to 0.09375
- w_gate: bfloat16 [32, 128, 4096], P('kv', 'tp'), may hold values from -0.09375 to 0.09375
- forget_floor: float32 [4096], P('kv'), may hold values from 0 to 0.95
- head_gain: float32 [128], P('tp'), may hold values from 0.1 to 1.9
- w_out: bfloat16 [4096, 4096], P('kv'), may hold values from -0.09375 to 0.09375
- state: float32 [128, 32, 128, 128], P(None, 'kv', 'tp'), may hold values from -12 to 12
- prev_forget: float32 [128, 4, 4096], P(None, None, 'kv'), may hold values from 0.2 to 1
- prev_input: bfloat16 [128, 4, 32, 128], P(None, None, 'kv', 'tp'), may hold values from -6 to 6
- accepted: int32 [128], replicated, may hold values from 0 to 4
Outputs:
- mixed: bfloat16 [128, 4, 4096], P(None, None, ('kv', 'tp'))
- new_state: float32 [128, 32, 128, 128], P(None, 'kv', 'tp')
All inputs are finite; a program needn't handle non-finite values.
Results may differ from a plain program's by a relative error of at most 0.019.
Values may be sent and summed in bfloat16 or wider, within the bound.
A program may use at most 128 MiB of HBM per device.

v0:
```python
import functools

import jax
import jax.numpy as jnp
from jax import lax
from jax.experimental import pallas as pl
from jax.experimental.pallas import tpu as pltpu
from jax.sharding import PartitionSpec as P

NORM_EPSILON = 1e-06
MESH = pl.DeviceIdType.MESH
VMEM_BYTES = 60 * 1024 * 1024
F32 = jnp.float32
BF16 = jnp.bfloat16


def contract(a, b, da, db):
    return lax.dot_general(a, b, (((da,), (db,)), ((), ())), preferred_element_type=F32)


def state_kernel(acc_ref, pf_ref, pv_ref, spread_ref, state_ref, new_ref, low_ref):
    prop, group, chans = pf_ref.shape
    heads, vals, keys = state_ref.shape[1:]
    wide = 8 * vals
    accepted = acc_ref[...]
    decay = jnp.ones((group, chans), F32)
    weights = [None] * prop
    for p in range(prop - 1, -1, -1):
        alive = p < accepted
        gate = pf_ref[p]
        weights[p] = jnp.where(alive, decay * (1.0 - gate), 0.0)
        decay = jnp.where(alive, decay * gate, decay)
    spread = [
        jnp.dot(pv_ref[p], spread_ref[...], preferred_element_type=F32) for p in range(prop)
    ]
    rows = lax.broadcasted_iota(jnp.int32, (8 * prop, wide), 0) % 8
    lanes = lax.broadcasted_iota(jnp.int32, (8 * prop, wide), 1) // vals
    mask = rows == lanes
    for g in range(group // 8):
        sl = slice(g * 8, g * 8 + 8)
        for h in range(heads):
            hk = slice(h * keys, (h + 1) * keys)
            lhs = jnp.concatenate(
                [spread[p][sl, h * wide : (h + 1) * wide] for p in range(prop)], axis=0
            )
            lhs = jnp.where(mask, lhs, 0.0).astype(BF16)
            rhs = jnp.concatenate([weights[p][sl, hk] for p in range(prop)], axis=0).astype(BF16)
            update = contract(lhs, rhs, 0, 0).reshape(8, vals, keys)
            new = decay[sl, hk][:, None, :] * state_ref[sl, h] + update
            new_ref[sl, h] = new
            low_ref[sl, h] = new.astype(BF16)


def update_state(accepted, prev_forget, prev_input, state):
    seqs, heads, vals, keys = state.shape
    prop = prev_forget.shape[1]
    group = 16
    pf = prev_forget.transpose(1, 0, 2)
    pv = prev_input.reshape(seqs, prop, heads * vals).transpose(1, 0, 2)
    r = jnp.arange(heads * vals)[:, None]
    c = jnp.arange(heads * 8 * vals)[None, :]
    spread = ((r // vals == c // (8 * vals)) & (r % vals == c % vals)).astype(BF16)
    block = (group, heads, vals, keys)
    return pl.pallas_call(
        state_kernel,
        grid=(seqs // group,),
        in_specs=[
            pl.BlockSpec((group, 1), lambda i: (i, 0)),
            pl.BlockSpec((prop, group, heads * keys), lambda i: (0, i, 0)),
            pl.BlockSpec((prop, group, heads * vals), lambda i: (0, i, 0)),
            pl.BlockSpec(spread.shape, lambda i: (0, 0)),
            pl.BlockSpec(block, lambda i: (i, 0, 0, 0)),
        ],
        out_specs=[
            pl.BlockSpec(block, lambda i: (i, 0, 0, 0)),
            pl.BlockSpec(block, lambda i: (i, 0, 0, 0)),
        ],
        out_shape=[
            jax.ShapeDtypeStruct(state.shape, F32),
            jax.ShapeDtypeStruct(state.shape, BF16),
        ],
        compiler_params=pltpu.CompilerParams(vmem_limit_bytes=VMEM_BYTES // 2),
        cost_estimate=pl.CostEstimate(
            flops=2 * 8 * prop * state.size, bytes_accessed=10 * state.size, transcendentals=0
        ),
    )(accepted.reshape(seqs, 1), pf, pv, spread, state)


def layer_kernel(
    kv_size,
    tp_size,
    tok_ref,
    gain_ref,
    floor_ref,
    hgain_ref,
    fold_ref,
    wq_hbm,
    wf_hbm,
    wi_hbm,
    wg_hbm,
    wo_hbm,
    st_hbm,
    out_ref,
    gath,
    wq,
    wf,
    wig,
    wo,
    st,
    acc,
    ss,
    qd,
    ho,
    pre,
    sq,
    rx,
    rsq,
    term,
    rt,
    w_sem,
    wo_sem,
    own_sem,
    z_send,
    a_send,
    b_send,
    d_send,
    slot_recv,
    d_recv,
    x_send,
    x_recv,
    s_send,
    s_recv,
    t_send,
    t_recv,
):
    n = kv_size * tp_size
    chips = n // 2
    zs = kv_size // 2
    kv = lax.axis_index("kv")
    tp = lax.axis_index("tp")
    me = kv * tp_size + tp
    z, y, x, c = kv // 2, kv % 2, tp // 2, tp % 2
    width = tok_ref.shape[1]
    rows = tok_ref.shape[0]
    seqs, heads, vals, keys = st_hbm.shape
    prop = rows // seqs
    hk = heads * keys
    hv = heads * vals
    features = n * width

    weight_copies = [
        pltpu.make_async_copy(wq_hbm, wq, w_sem.at[0]),
        pltpu.make_async_copy(wf_hbm, wf, w_sem.at[1]),
        pltpu.make_async_copy(wi_hbm, wig.at[pl.ds(0, hv)], w_sem.at[2]),
        pltpu.make_async_copy(wg_hbm, wig.at[pl.ds(hv, hv)], w_sem.at[3]),
    ]
    state_copy = pltpu.make_async_copy(st_hbm, st, w_sem.at[4])
    out_copies = [
        pltpu.make_async_copy(
            wo_hbm.at[pl.ds(h * keys + j * vals, vals)],
            wo.at[pl.ds((j * heads + h) * vals, vals)],
            wo_sem.at[h * tp_size + j],
        )
        for h in range(heads)
        for j in range(tp_size)
    ]

    def columns(zr, fy, fx, core):
        oz = (z + zr) % zs
        oy = y + fy * (1 - 2 * y)
        ox = x + fx * (1 - 2 * x)
        index = (oz * 2 + oy) * tp_size + ox * 2 + core
        return pl.ds(pl.multiple_of(index * width, width), width)

    own = pltpu.make_async_copy(tok_ref, gath.at[:, columns(0, 0, 0, c)], own_sem)
    own.start()

    barrier = pltpu.get_barrier_semaphore()

    @pl.loop(1, n)
    def _(d):
        other = (me + d) % n
        pl.semaphore_signal(
            barrier,
            inc=1,
            device_id=(other // tp_size, other % tp_size),
            device_id_type=MESH,
        )

    own.wait()
    pl.semaphore_wait(barrier, n - 1)

    def remote(view, send, recv, target):
        return pltpu.make_async_remote_copy(
            src_ref=view,
            dst_ref=view,
            send_sem=send,
            recv_sem=recv,
            device_id=target,
            device_id_type=MESH,
        )

    a_peer = (kv + (1 - c) * (1 - 2 * y), tp + c * (1 - 2 * x) * 2)
    b_peer = (kv + c * (1 - 2 * y), tp + (1 - c) * (1 - 2 * x) * 2)
    partner = (kv, tp + 1 - 2 * c)

    def flips(ar, br):
        return ar * (1 - c) + br * c, ar * c + br * (1 - c)

    def view(zr, ar, br):
        fy, fx = flips(ar, br)
        return gath.at[:, columns(zr, fy, fx, c)]

    def slot(zr, ar, br):
        fy, fx = flips(ar, br)
        return zr * 4 + fy * 2 + fx

    def to_z(zr):
        return remote(
            view(0, 0, 0),
            z_send.at[zr],
            slot_recv.at[zr * 4],
            (((z + zs - zr) % zs) * 2 + y, tp),
        )

    def to_a(zr):
        return remote(view(zr, 0, 0), a_send.at[zr], slot_recv.at[slot(zr, 1, 0)], a_peer)

    def to_b(zr, ar):
        return remote(
            view(zr, ar, 0), b_send.at[zr * 2 + ar], slot_recv.at[slot(zr, ar, 1)], b_peer
        )

    def to_partner(zr, ar, br):
        s = slot(zr, ar, br)
        return remote(view(zr, ar, br), d_send.at[s], d_recv.at[s], partner)

    def arrived(zr, ar, br):
        remote(
            view(zr, ar, br), z_send.at[0], slot_recv.at[slot(zr, ar, br)], partner
        ).wait_recv()

    for zr in range(1, zs):
        to_z(zr).start()
    to_a(0).start()
    to_b(0, 0).start()
    for copy in weight_copies:
        copy.start()
    to_partner(0, 0, 0).start()
    state_copy.start()
    for copy in out_copies:
        copy.start()
    acc[...] = jnp.zeros_like(acc)
    ss[...] = jnp.zeros_like(ss)
    ones = jnp.ones((2 * width, ss.shape[1]), BF16)
    for copy in weight_copies:
        copy.wait()

    @pl.loop(0, zs)
    def _(zr):
        @pl.when(zr > 0)
        def _():
            arrived(zr, 0, 0)
            to_a(zr).start()
            to_b(zr, 0).start()
            to_partner(zr, 0, 0).start()

        arrived(zr, 1, 0)
        to_b(zr, 1).start()
        to_partner(zr, 1, 0).start()
        arrived(zr, 0, 1)
        to_partner(zr, 0, 1).start()
        arrived(zr, 1, 1)
        to_partner(zr, 1, 1).start()

        @pl.loop(0, 4)
        def _(f):
            fy, fx = f // 2, f % 2
            other = columns(zr, fy, fx, 1 - c)
            remote(gath.at[:, other], z_send.at[0], d_recv.at[zr * 4 + f], partner).wait_recv()
            oz = (z + zr) % zs
            index = (oz * 2 + y + fy * (1 - 2 * y)) * (tp_size // 2) + x + fx * (1 - 2 * x)
            pair = pl.ds(pl.multiple_of(index * 2 * width, 2 * width), 2 * width)
            raw = gath[:, pair].astype(F32)
            ss[...] += jnp.dot((raw * raw).astype(BF16), ones, preferred_element_type=F32)
            lhs = (raw * gain_ref[:, pair]).astype(BF16)
            acc[:, 0:hk] += jnp.dot(lhs, wq[pair, :], preferred_element_type=F32)
            acc[:, hk : 2 * hk] += jnp.dot(lhs, wf[pair, :], preferred_element_type=F32)
            acc[:, 2 * hk :] += contract(lhs, wig[:, pair], 1, 1)

    for t in range(prop):
        r = slice(t * seqs, (t + 1) * seqs)
        scale = lax.rsqrt(ss[r, :] * (1.0 / features) + NORM_EPSILON)
        for j in range(acc.shape[1] // 128):
            cs = slice(j * 128, (j + 1) * 128)
            value = (acc[r, cs] * scale).astype(BF16).astype(F32)
            if hk <= j * 128 < 2 * hk:
                fs = slice(j * 128 - hk, j * 128 - hk + 128)
                floor = floor_ref[:, fs]
                value = floor + (1.0 - floor) * jax.nn.sigmoid(value)
            acc[r, cs] = value

    def part(t, first, size):
        return acc[t * seqs : (t + 1) * seqs, first : first + size]

    run = None
    for t in range(prop):
        gate = part(t, hk, hk)
        run = gate if run is None else run * gate
        qd[t] = part(t, 0, hk) * run
    for t in range(prop):
        total = None
        back = None
        for u in range(t, -1, -1):
            near = 1.0 - part(u, hk, hk)
            reach = part(t, 0, hk) if back is None else part(t, 0, hk) * back
            score = jnp.dot((reach * near).astype(BF16), fold_ref[...], preferred_element_type=F32)
            piece = score * part(u, 2 * hk, hv)
            total = piece if total is None else total + piece
            gate = part(u, hk, hk)
            back = gate if back is None else back * gate
        ho[t] = total

    state_copy.wait()
    wide = 8 * vals
    mask = (lax.broadcasted_iota(jnp.int32, (8 * prop, wide), 0) % 8) == (
        lax.broadcasted_iota(jnp.int32, (8 * prop, wide), 1) // vals
    )
    lane_head = lax.broadcasted_iota(jnp.int32, (8 * prop, hv), 1) // vals

    @pl.loop(0, seqs // 8)
    def _(g):
        group = pl.ds(pl.multiple_of(g * 8, 8), 8)
        result = jnp.zeros((8 * prop, hv), F32)
        for h in range(heads):
            lhs = qd[:, group, h * keys : (h + 1) * keys].reshape(8 * prop, keys).astype(BF16)
            rhs = st[group, h].reshape(wide, keys)
            o = jnp.where(mask, contract(lhs, rhs, 1, 1), 0.0)
            folded = o[:, :hv]
            for k in range(1, wide // hv):
                folded = folded + o[:, k * hv : (k + 1) * hv]
            step = hv // 2
            while step >= vals:
                folded = folded + pltpu.roll(folded, step, 1)
                step //= 2
            result = jnp.where(lane_head == h, folded, result)
        ho[:, group, :] += result.reshape(prop, 8, hv)

    pick = (
        lax.broadcasted_iota(jnp.int32, (8, hv), 0)
        == lax.broadcasted_iota(jnp.int32, (8, hv), 1) // vals
    ).astype(BF16)
    for t in range(prop):
        raw = ho[t]
        gate = part(t, 2 * hk + hv, hv)
        pre[t] = (raw * hgain_ref[...] * (gate * jax.nn.sigmoid(gate))).astype(BF16)
        sq[t] = contract(pick, (raw * raw).astype(BF16), 1, 1)

    exchanges = []
    for d in range(1, tp_size):
        to = (tp + d) % tp_size
        for src, dst, send, recv in ((pre, rx, x_send, x_recv), (sq, rsq, s_send, s_recv)):
            copy = pltpu.make_async_remote_copy(
                src_ref=src.at[to],
                dst_ref=dst.at[tp],
                send_sem=send.at[d],
                recv_sem=recv.at[d],
                device_id=(kv, to),
                device_id_type=MESH,
            )
            copy.start()
            exchanges.append(copy)
    rx[tp] = pre[tp]
    rsq[tp] = sq[tp]
    for copy in out_copies:
        copy.wait()
    for copy in exchanges:
        copy.wait()

    squares = rsq[0]
    for j in range(1, tp_size):
        squares = squares + rsq[j]
    factor = lax.rsqrt(squares * (1.0 / keys) + NORM_EPSILON)
    place = (
        lax.broadcasted_iota(jnp.int32, (8, tp_size * hv), 0)
        == (lax.broadcasted_iota(jnp.int32, (8, tp_size * hv), 1) // vals) % heads
    ).astype(BF16)
    high = factor.astype(BF16)
    low = (factor - high.astype(F32)).astype(BF16)
    factors = contract(high, place, 0, 0) + contract(low, place, 0, 0)
    flat = jnp.concatenate([rx[j] for j in range(tp_size)], axis=1).astype(F32)
    flat = (flat * factors).astype(BF16)

    home = me // 2

    def to_owner(k, core):
        chip = (home + k) % chips
        dest = chip * 2 + core
        return pltpu.make_async_remote_copy(
            src_ref=term.at[dest],
            dst_ref=rt.at[tp * kv_size + kv],
            send_sem=t_send.at[k * 2 + core],
            recv_sem=t_recv.at[k * 2 + c],
            device_id=(dest // tp_size, dest % tp_size),
            device_id_type=MESH,
        )

    @pl.loop(0, chips)
    def _(i):
        k = (i + 1) % chips
        chip = (home + k) % chips
        cols = pl.ds(pl.multiple_of(chip * 2 * width, 2 * width), 2 * width)
        pair = jnp.dot(flat, wo[:, cols], preferred_element_type=F32).astype(BF16)
        term[chip * 2] = pair[:, :width]
        term[chip * 2 + 1] = pair[:, width:]

        @pl.when(k > 0)
        def _():
            to_owner(k, 0).start()
            to_owner(k, 1).start()

    to_owner(0, 1 - c).start()
    rt[tp * kv_size + kv] = term[me]

    for zr in range(1, zs):
        to_z(zr).wait_send()
    for zr in range(zs):
        to_a(zr).wait_send()
        for ar in range(2):
            to_b(zr, ar).wait_send()
            for br in range(2):
                to_partner(zr, ar, br).wait_send()

    def landed(k, core):
        source = ((home + chips - k) % chips) * 2 + core
        block = rt.at[(source % tp_size) * kv_size + source // tp_size]
        pltpu.make_async_remote_copy(
            src_ref=block,
            dst_ref=block,
            send_sem=t_send.at[k * 2 + core],
            recv_sem=t_recv.at[k * 2 + core],
            device_id=partner,
            device_id_type=MESH,
        ).wait_recv()

    landed(0, 1 - c)
    to_owner(0, 1 - c).wait_send()

    @pl.loop(1, chips)
    def _(k):
        landed(k, 0)
        landed(k, 1)
        to_owner(k, 0).wait_send()
        to_owner(k, 1).wait_send()

    for j in range(tp_size):
        total = rt[j * kv_size].astype(F32)
        for i in range(1, kv_size):
            total = total + rt[j * kv_size + i].astype(F32)
        out_ref[j * seqs : (j + 1) * seqs, :] = total.astype(BF16)


def fused(
    kv_size,
    tp_size,
    tokens,
    input_norm_gain,
    w_query,
    w_forget,
    w_input,
    w_gate,
    forget_floor,
    head_gain,
    w_out,
    state,
    prev_forget,
    prev_input,
    accepted,
):
    seqs, prop, width = tokens.shape
    heads, vals, keys = state.shape[1:]
    n = kv_size * tp_size
    rows, features = seqs * prop, n * width
    hk, hv = heads * keys, heads * vals
    new_state, low_state = update_state(accepted, prev_forget, prev_input, state)
    fold = (jnp.arange(hk)[:, None] // keys == jnp.arange(hv)[None, :] // vals).astype(BF16)
    vmem = pl.BlockSpec(memory_space=pltpu.VMEM)
    hbm = pl.BlockSpec(memory_space=pl.ANY)
    dma = pltpu.SemaphoreType.DMA
    slots = kv_size * tp_size // 2
    out = pl.pallas_call(
        functools.partial(layer_kernel, kv_size, tp_size),
        out_shape=jax.ShapeDtypeStruct((rows, width), BF16),
        in_specs=[vmem] * 5 + [hbm] * 6,
        out_specs=vmem,
        scratch_shapes=[
            pltpu.VMEM((rows, features), BF16),
            pltpu.VMEM((features, hk), BF16),
            pltpu.VMEM((features, hk), BF16),
            pltpu.VMEM((2 * hv, features), BF16),
            pltpu.VMEM((hk, features), BF16),
            pltpu.VMEM((seqs, heads, vals, keys), BF16),
            pltpu.VMEM((rows, 2 * hk + 2 * hv), F32),
            pltpu.VMEM((rows, 128), F32),
            pltpu.VMEM((prop, seqs, hk), F32),
            pltpu.VMEM((prop, seqs, hv), F32),
            pltpu.VMEM((prop, seqs, hv), BF16),
            pltpu.VMEM((prop, 8, seqs), F32),
            pltpu.VMEM((tp_size, seqs, hv), BF16),
            pltpu.VMEM((tp_size, 8, seqs), F32),
            pltpu.VMEM((n, seqs, width), BF16),
            pltpu.VMEM((n, seqs, width), BF16),
            dma((5,)),
            dma((heads * tp_size,)),
            dma,
            dma((kv_size // 2,)),
            dma((kv_size // 2,)),
            dma((kv_size,)),
            dma((slots,)),
            dma((slots,)),
            dma((slots,)),
            dma((tp_size,)),
            dma((tp_size,)),
            dma((tp_size,)),
            dma((tp_size,)),
            dma((n,)),
            dma((n,)),
        ],
        compiler_params=pltpu.CompilerParams(
            collective_id=0, has_side_effects=True, vmem_limit_bytes=VMEM_BYTES
        ),
        cost_estimate=pl.CostEstimate(
            flops=2 * rows * features * (2 * hk + 3 * hv),
            bytes_accessed=2 * features * (3 * hk + 2 * hv),
            transcendentals=0,
        ),
    )(
        tokens.transpose(1, 0, 2).reshape(rows, width),
        input_norm_gain.reshape(1, features),
        forget_floor.reshape(1, hk),
        jnp.tile(head_gain, heads).reshape(1, hv),
        fold,
        w_query,
        w_forget,
        w_input.reshape(hv, features),
        w_gate.reshape(hv, features),
        w_out,
        low_state,
    )
    return out.reshape(prop, seqs, width).transpose(1, 0, 2), new_state


def fits(kv_size, tp_size, tokens, state):
    seqs, prop, width = tokens.shape
    heads, vals, keys = state.shape[1:]
    return (
        kv_size % 2 == 0
        and tp_size == 4
        and prop == tp_size
        and width == 128
        and seqs == 128
        and keys == 128
        and heads * vals == 128
        and vals % 32 == 0
        and heads <= 8
    )


def rms_scale(values, gain):
    return (
        values * lax.rsqrt(jnp.mean(values * values, axis=-1, keepdims=True) + NORM_EPSILON) * gain
    )


def by_rows(normed, weight):
    return lax.dot_general(
        normed, weight, (((1,), (1,)), ((), ())), preferred_element_type=jnp.float32
    )


def general(
    tokens,
    input_norm_gain,
    w_query,
    w_forget,
    w_input,
    w_gate,
    forget_floor,
    head_gain,
    w_out,
    state,
    prev_forget,
    prev_input,
    accepted,
):
    seq_count = tokens.shape[0]
    proposals = tokens.shape[1]
    whole = lax.all_gather(tokens, ("kv", "tp"), axis=2, tiled=True)
    widths = whole.shape[2]
    row_count = seq_count * proposals
    normed = (
        rms_scale(whole.astype(jnp.float32), input_norm_gain)
        .astype(jnp.bfloat16)
        .reshape(row_count, widths)
    )
    heads_local = state.shape[1]
    value_local = state.shape[2]
    head_size = state.shape[3]
    group_members = lax.axis_size("tp")
    queries = jnp.dot(normed, w_query, preferred_element_type=jnp.float32).astype(jnp.bfloat16)
    forget_raw = jnp.dot(normed, w_forget, preferred_element_type=jnp.float32).astype(jnp.bfloat16)
    input_proj = by_rows(normed, w_input.reshape(heads_local * value_local, widths)).astype(
        jnp.bfloat16
    )
    gate_raw = by_rows(normed, w_gate.reshape(heads_local * value_local, widths)).astype(
        jnp.bfloat16
    )
    head_shape = (seq_count, proposals, heads_local, head_size)
    value_shape = (seq_count, proposals, heads_local, value_local)
    forget = forget_floor + (1.0 - forget_floor) * jax.nn.sigmoid(forget_raw.astype(jnp.float32))
    forget = forget.reshape(head_shape)
    log_forget = jnp.log(forget)
    keys_now = 1.0 - forget
    values_now = input_proj.astype(jnp.float32).reshape(value_shape)
    query_vector = queries.astype(jnp.float32).reshape(head_shape)
    previous = prev_forget.reshape(head_shape)
    prev_values = prev_input.astype(jnp.float32)
    alive_mask = (jnp.arange(proposals)[None, :] < accepted[:, None])[:, :, None, None]
    prev_log = jnp.where(alive_mask, jnp.log(previous), 0.0)
    prev_cum = jnp.cumsum(prev_log, axis=1)
    prev_total = prev_cum[:, -1]
    weights_prev = jnp.where(
        alive_mask, jnp.exp(prev_total[:, None] - prev_cum) * (1.0 - previous), 0.0
    )
    new_state = jnp.exp(prev_total)[:, :, None, :] * state + jnp.einsum(
        "sphk,sphv->shvk", weights_prev, prev_values
    )
    decay_cum = jnp.cumsum(log_forget, axis=1)
    carried = jnp.einsum("sthk,shvk->sthv", query_vector * jnp.exp(decay_cum), new_state)
    triangle = jnp.tril(jnp.ones((proposals, proposals), dtype=bool))[None, :, :, None, None]
    spread = jnp.where(triangle, decay_cum[:, :, None] - decay_cum[:, None, :], 0.0)
    relative = jnp.where(triangle, jnp.exp(spread), 0.0)
    scores = jnp.einsum("sthk,suhk,stuhk->stuh", query_vector, keys_now, relative)
    heads_out = carried + jnp.einsum("stuh,suhv->sthv", scores, values_now)
    square_sum = lax.psum(jnp.sum(heads_out * heads_out, axis=-1), "tp")
    norm_factor = lax.rsqrt(square_sum / head_size + NORM_EPSILON)
    gate_heads = gate_raw.astype(jnp.float32).reshape(value_shape)
    hidden = (heads_out * norm_factor[..., None] * head_gain * jax.nn.silu(gate_heads)).astype(
        jnp.bfloat16
    )
    hidden_heads = hidden.reshape(row_count, heads_local, value_local)
    regrouped = lax.all_to_all(hidden_heads, "tp", split_axis=0, concat_axis=2, tiled=True)
    flat = regrouped.reshape(row_count // group_members, heads_local * head_size)
    term = jnp.dot(flat, w_out, preferred_element_type=jnp.float32)
    summed = lax.psum_scatter(term.astype(jnp.bfloat16), "kv", scatter_dimension=1, tiled=True)
    placed = lax.all_to_all(summed, "tp", split_axis=1, concat_axis=0, tiled=True)
    mixed = placed.reshape(seq_count, proposals, -1)
    return (mixed, new_state)


def solution(mesh):
    placed = (
        P(None, None, ("kv", "tp")),
        P(),
        P(None, "kv"),
        P(None, "kv"),
        P("kv", "tp", None),
        P("kv", "tp", None),
        P("kv"),
        P("tp"),
        P("kv", None),
        P(None, "kv", "tp", None),
        P(None, None, "kv"),
        P(None, None, "kv", "tp"),
        P(),
    )
    kv_size, tp_size = mesh.shape["kv"], mesh.shape["tp"]

    def body(*args):
        if fits(kv_size, tp_size, args[0], args[9]):
            return fused(kv_size, tp_size, *args)
        return general(*args)

    return jax.shard_map(
        body,
        mesh=mesh,
        in_specs=placed,
        out_specs=(P(None, None, ("kv", "tp")), P(None, "kv", "tp", None)),
        check_vma=False,
    )
```

profile of v0, /device:TPU:15, one launch (start us, length us, event | category | flops | bytes accessed | tf_op | source)
XLA Modules:
  0.0 107.0 jit_solution(11234099793308073582)
XLA Ops:
  0.6 0.1 and_convert_fusion.spread_ref
  0.8 1.6 %copy.27 = f32[128,4,512]{2,0,1:T(8,128)S(1)} copy(f32[128,4,512]{2,1,0:T(4,128)} %param.23) | data formatting | bytes 2097152 | tf_op args[10]
  2.4 1.0 copy.22
  3.4 0.8 copy.23.acc_ref
  4.2 0.0 copy-start
  4.2 3.4 %copy-done = f32[128,4,32,128]{3,2,1,0:T(8,128)S(1)} copy-done((f32[128,4,32,128]{3,2,1,0:T(8,128)S(1)}, f32[128,4,32,128]{3,2,1,0:T(8,128)}, u32[]{:S(2)}) %copy-start) | copy-done | bytes 8388632
  7.5 0.0 copy-start.2
  7.6 0.0 copy-start.3
  7.6 7.0 %shard_map.140 = (f32[128,4,32,128]{3,2,1,0:T(8,128)}, bf16[128,4,32,128]{3,2,1,0:T(8,128)(2,1)S(1)}) custom-call(s32[128,1]{1,0:T(8,128)S(1)} %copy.23.acc_ref, f32[4,128,512]{2,1,0:T(8,128)S(1)} %bitcast.16, bf16[4,128,128]{2,1,0:T(8,128)(2,1)S(1)} %bitcast.17, bf16[128,1024]{1,0:T(8,128)(2,1)S(1)} %and_convert_fusion.spread_ref, ...), custom_call_target="tpu_custom_call" | custom-call | flops 134217728 | bytes 20971520 | tf_op jit(solution)/shard_map/pallas_call | solution.py:64
  14.5 0.0 copy-start.1
  14.5 1.9 %copy-done.1 = bf16[128,4,32,128]{3,2,1,0:T(8,128)(2,1)} copy-done((bf16[128,4,32,128]{3,2,1,0:T(8,128)(2,1)}, bf16[128,4,32,128]{3,2,1,0:T(8,128)(2,1)S(1)}, u32[]{:S(2)}) %copy-start.1) | copy-done | bytes 4194328
  16.5 0.8 compare_convert_fusion.fold_ref
  17.3 0.0 copy-done.2
  17.3 0.7 copy.20
  17.9 0.0 copy-done.3
  17.9 0.7 reshape_tile.3.hgain_ref
  18.6 86.7 %shard_map.141 = bf16[512,128]{1,0:T(8,128)(2,1)} custom-call(bf16[512,128]{1,0:T(8,128)(2,1)} %bitcast.21, f32[1,4096]{1,0:T(1,128)} %bitcast.26, f32[1,512]{1,0:T(1,128)} %bitcast.27, f32[1,128]{1,0:T(1,128)} %reshape_tile.3.hgain_ref, bf16[512,128]{1,0:T(8,128)(2,1)} %compare_convert_fusion.fold_ref, bf16[4096,512]{1,0:T(8,128)(2,1)} %wq_hbm.1, ...), custom_call_target="tpu_custom_call" | custom-call | flops 5905580032 | bytes 14680064 | tf_op jit(solution)/shard_map/pallas_call | solution.py:491
  105.4 1.7 %copy.28 = bf16[4,128,128]{2,0,1:T(4,128)(2,1)} copy(bf16[4,128,128]{2,1,0:T(8,128)(2,1)} %bitcast.22) | data formatting | bytes 262144 | tf_op jit(solution)/shard_map/reshape | solution.py:550
  (4 shorter events, 0.0 us)
Async XLA Ops:
  4.2 3.4 %copy-start = (f32[128,4,32,128]{3,2,1,0:T(8,128)S(1)}, f32[128,4,32,128]{3,2,1,0:T(8,128)}, u32[]{:S(2)}) copy-start(f32[128,4,32,128]{3,2,1,0:T(8,128)} %state_ref.1) | copy-start | bytes 25165828
  7.5 9.7 %copy-start.2 = (bf16[128,4,128]{2,1,0:T(4,128)(2,1)S(1)}, bf16[128,4,128]{2,1,0:T(4,128)(2,1)}, u32[]{:S(2)}) copy-start(bf16[128,4,128]{2,1,0:T(4,128)(2,1)} %param.13) | copy-start | bytes 393220
  7.6 10.4 %copy-start.3 = (f32[32]{0:T(128)S(1)}, f32[32]{0:T(128)}, u32[]{:S(2)}) copy-start(f32[32]{0:T(128)} %param.20) | copy-start | bytes 388
  14.5 1.9 %copy-start.1 = (bf16[128,4,32,128]{3,2,1,0:T(8,128)(2,1)}, bf16[128,4,32,128]{3,2,1,0:T(8,128)(2,1)S(1)}, u32[]{:S(2)}) copy-start(bf16[128,4,32,128]{3,2,1,0:T(8,128)(2,1)S(1)} %get-tuple-element.4.st_hbm) | copy-start | bytes 12582916
where the time goes:
time: 107 us
  Pallas kernels  93.7 us (88%)
  local copies, waits for them, and re-layouts  11.7 us (11%)
    pallas_call x1, Pallas kernels, fused(): pl.pallas_call(functools.partial(layer_kernel, kv_size, tp_size), out_sha...  86.7 us
    pallas_call x1, Pallas kernels, update_state(): pl.pallas_call(state_kernel, grid=(seqs // group,), in_specs=[pl.BlockSpe...  6.97 us
    unnamed x9, local copies, waits for them, and re-layouts  6.89 us

commit v1 on v0

--- a/solution.py
+++ b/solution.py
@@ -79,7 +79,7 @@
             jax.ShapeDtypeStruct(state.shape, F32),
             jax.ShapeDtypeStruct(state.shape, BF16),
         ],
-        compiler_params=pltpu.CompilerParams(vmem_limit_bytes=VMEM_BYTES // 2),
+        compiler_params=pltpu.CompilerParams(vmem_limit_bytes=VMEM_BYTES),
         cost_estimate=pl.CostEstimate(
             flops=2 * 8 * prop * state.size, bytes_accessed=10 * state.size, transcendentals=0
         ),
@@ -93,7 +93,6 @@
     gain_ref,
     floor_ref,
     hgain_ref,
-    fold_ref,
     wq_hbm,
     wf_hbm,
     wi_hbm,
@@ -116,6 +115,10 @@
     rx,
     rsq,
     term,
+    mine,
+    half,
+    quarter,
+    done,
     rt,
     w_sem,
     wo_sem,
@@ -134,7 +137,6 @@
     t_recv,
 ):
     n = kv_size * tp_size
-    chips = n // 2
     zs = kv_size // 2
     kv = lax.axis_index("kv")
     tp = lax.axis_index("tp")
@@ -308,13 +310,17 @@
         gate = part(t, hk, hk)
         run = gate if run is None else run * gate
         qd[t] = part(t, 0, hk) * run
+    fold = (
+        lax.broadcasted_iota(jnp.int32, (hk, hv), 0) // keys
+        == lax.broadcasted_iota(jnp.int32, (hk, hv), 1) // vals
+    ).astype(BF16)
     for t in range(prop):
         total = None
         back = None
         for u in range(t, -1, -1):
             near = 1.0 - part(u, hk, hk)
             reach = part(t, 0, hk) if back is None else part(t, 0, hk) * back
-            score = jnp.dot((reach * near).astype(BF16), fold_ref[...], preferred_element_type=F32)
+            score = jnp.dot((reach * near).astype(BF16), fold, preferred_element_type=F32)
             piece = score * part(u, 2 * hk, hv)
             total = piece if total is None else total + piece
             gate = part(u, hk, hk)
@@ -328,7 +334,7 @@
     )
     lane_head = lax.broadcasted_iota(jnp.int32, (8 * prop, hv), 1) // vals
 
-    @pl.loop(0, seqs // 8)
+    @pl.loop(0, seqs // 8, unroll=2)
     def _(g):
         group = pl.ds(pl.multiple_of(g * 8, 8), 8)
         result = jnp.zeros((8 * prop, hv), F32)
@@ -350,10 +356,11 @@
         lax.broadcasted_iota(jnp.int32, (8, hv), 0)
         == lax.broadcasted_iota(jnp.int32, (8, hv), 1) // vals
     ).astype(BF16)
+    head_gain = jnp.concatenate([hgain_ref[...]] * heads, axis=1)
     for t in range(prop):
         raw = ho[t]
         gate = part(t, 2 * hk + hv, hv)
-        pre[t] = (raw * hgain_ref[...] * (gate * jax.nn.sigmoid(gate))).astype(BF16)
+        pre[t] = (raw * head_gain * (gate * jax.nn.sigmoid(gate))).astype(BF16)
         sq[t] = contract(pick, (raw * raw).astype(BF16), 1, 1)
 
     exchanges = []
@@ -391,36 +398,80 @@
     flat = jnp.concatenate([rx[j] for j in range(tp_size)], axis=1).astype(F32)
     flat = (flat * factors).astype(BF16)
 
-    home = me // 2
-
-    def to_owner(k, core):
-        chip = (home + k) % chips
-        dest = chip * 2 + core
+    y_peer = (kv + 1 - 2 * y, tp)
+    order = list(range(1, zs)) + [0]
+
+    def blocks(dz, side):
+        start = (((z + dz) % zs) * 2 + side) * tp_size
+        return pl.ds(start, tp_size)
+
+    def to_y(dz):
         return pltpu.make_async_remote_copy(
-            src_ref=term.at[dest],
-            dst_ref=rt.at[tp * kv_size + kv],
-            send_sem=t_send.at[k * 2 + core],
-            recv_sem=t_recv.at[k * 2 + c],
-            device_id=(dest // tp_size, dest % tp_size),
+            src_ref=term.at[blocks(dz, 1 - y)],
+            dst_ref=half.at[dz],
+            send_sem=t_send.at[dz],
+            recv_sem=t_recv.at[dz],
+            device_id=y_peer,
             device_id_type=MESH,
         )
 
-    @pl.loop(0, chips)
-    def _(i):
-        k = (i + 1) % chips
-        chip = (home + k) % chips
-        cols = pl.ds(pl.multiple_of(chip * 2 * width, 2 * width), 2 * width)
-        pair = jnp.dot(flat, wo[:, cols], preferred_element_type=F32).astype(BF16)
-        term[chip * 2] = pair[:, :width]
-        term[chip * 2 + 1] = pair[:, width:]
-
-        @pl.when(k > 0)
-        def _():
-            to_owner(k, 0).start()
-            to_owner(k, 1).start()
-
-    to_owner(0, 1 - c).start()
-    rt[tp * kv_size + kv] = term[me]
+    def along_z(dz):
+        return pltpu.make_async_remote_copy(
+            src_ref=term.at[blocks(dz, y)],
+            dst_ref=quarter.at[dz],
+            send_sem=t_send.at[zs + dz],
+            recv_sem=t_recv.at[zs + dz],
+            device_id=(((z + dz) % zs) * 2 + y, tp),
+            device_id_type=MESH,
+        )
+
+    def product(dz, side):
+        first = (((z + dz) % zs) * 2 + side) * tp_size * width
+        cols = pl.ds(pl.multiple_of(first, tp_size * width), tp_size * width)
+        return jnp.dot(flat, wo[:, cols], preferred_element_type=F32)
+
+    for dz in order:
+        away = product(dz, 1 - y).astype(BF16)
+        base = (((z + dz) % zs) * 2 + 1 - y) * tp_size
+        for j in range(tp_size):
+            term[base + j] = away[:, j * width : (j + 1) * width]
+        to_y(dz).start()
+    for dz in order:
+        mine[dz] = product(dz, y)
+    for dz in order:
+        to_y(dz).wait_recv()
+        base = (((z + dz) % zs) * 2 + y) * tp_size
+        for j in range(tp_size):
+            cs = slice(j * width, (j + 1) * width)
+            total = mine[dz, :, cs] + half[dz, j].astype(F32)
+            if dz > 0:
+                term[base + j] = total.astype(BF16)
+            else:
+                mine[dz, :, cs] = total
+        if dz > 0:
+            along_z(dz).start()
+    for dz in range(1, zs):
+        along_z(dz).wait_recv()
+    for j in range(tp_size):
+        total = mine[0, :, j * width : (j + 1) * width]
+        for dz in range(1, zs):
+            total = total + quarter[dz, j].astype(F32)
+        done[j] = total.astype(BF16)
+
+    finals = []
+    for d in range(1, tp_size):
+        to = (tp + d) % tp_size
+        copy = pltpu.make_async_remote_copy(
+            src_ref=done.at[to],
+            dst_ref=rt.at[tp],
+            send_sem=t_send.at[2 * zs + d],
+            recv_sem=t_recv.at[2 * zs + d],
+            device_id=(kv, to),
+            device_id_type=MESH,
+        )
+        copy.start()
+        finals.append(copy)
+    rt[tp] = done[tp]
 
     for zr in range(1, zs):
         to_z(zr).wait_send()
@@ -431,33 +482,14 @@
             for br in range(2):
                 to_partner(zr, ar, br).wait_send()
 
-    def landed(k, core):
-        source = ((home + chips - k) % chips) * 2 + core
-        block = rt.at[(source % tp_size) * kv_size + source // tp_size]
-        pltpu.make_async_remote_copy(
-            src_ref=block,
-            dst_ref=block,
-            send_sem=t_send.at[k * 2 + core],
-            recv_sem=t_recv.at[k * 2 + core],
-            device_id=partner,
-            device_id_type=MESH,
-        ).wait_recv()
-
-    landed(0, 1 - c)
-    to_owner(0, 1 - c).wait_send()
-
-    @pl.loop(1, chips)
-    def _(k):
-        landed(k, 0)
-        landed(k, 1)
-        to_owner(k, 0).wait_send()
-        to_owner(k, 1).wait_send()
-
+    for dz in range(zs):
+        to_y(dz).wait_send()
+        if dz > 0:
+            along_z(dz).wait_send()
+    for copy in finals:
+        copy.wait()
     for j in range(tp_size):
-        total = rt[j * kv_size].astype(F32)
-        for i in range(1, kv_size):
-            total = total + rt[j * kv_size + i].astype(F32)
-        out_ref[j * seqs : (j + 1) * seqs, :] = total.astype(BF16)
+        out_ref[j * seqs : (j + 1) * seqs, :] = rt[j]
 
 
 def fused(
@@ -483,7 +515,6 @@
     rows, features = seqs * prop, n * width
     hk, hv = heads * keys, heads * vals
     new_state, low_state = update_state(accepted, prev_forget, prev_input, state)
-    fold = (jnp.arange(hk)[:, None] // keys == jnp.arange(hv)[None, :] // vals).astype(BF16)
     vmem = pl.BlockSpec(memory_space=pltpu.VMEM)
     hbm = pl.BlockSpec(memory_space=pl.ANY)
     dma = pltpu.SemaphoreType.DMA
@@ -491,7 +522,7 @@
     out = pl.pallas_call(
         functools.partial(layer_kernel, kv_size, tp_size),
         out_shape=jax.ShapeDtypeStruct((rows, width), BF16),
-        in_specs=[vmem] * 5 + [hbm] * 6,
+        in_specs=[vmem] * 4 + [hbm] * 6,
         out_specs=vmem,
         scratch_shapes=[
             pltpu.VMEM((rows, features), BF16),
@@ -509,7 +540,11 @@
             pltpu.VMEM((tp_size, seqs, hv), BF16),
             pltpu.VMEM((tp_size, 8, seqs), F32),
             pltpu.VMEM((n, seqs, width), BF16),
-            pltpu.VMEM((n, seqs, width), BF16),
+            pltpu.VMEM((kv_size // 2, seqs, tp_size * width), F32),
+            pltpu.VMEM((kv_size // 2, tp_size, seqs, width), BF16),
+            pltpu.VMEM((kv_size // 2, tp_size, seqs, width), BF16),
+            pltpu.VMEM((tp_size, seqs, width), BF16),
+            pltpu.VMEM((tp_size, seqs, width), BF16),
             dma((5,)),
             dma((heads * tp_size,)),
             dma,
@@ -523,8 +558,8 @@
             dma((tp_size,)),
             dma((tp_size,)),
             dma((tp_size,)),
-            dma((n,)),
-            dma((n,)),
+            dma((kv_size + tp_size,)),
+            dma((kv_size + tp_size,)),
         ],
         compiler_params=pltpu.CompilerParams(
             collective_id=0, has_side_effects=True, vmem_limit_bytes=VMEM_BYTES
@@ -538,8 +573,7 @@
         tokens.transpose(1, 0, 2).reshape(rows, width),
         input_norm_gain.reshape(1, features),
         forget_floor.reshape(1, hk),
-        jnp.tile(head_gain, heads).reshape(1, hv),
-        fold,
+        head_gain.reshape(1, vals),
         w_query,
         w_forget,
         w_input.reshape(hv, features),

time: 107 us -> 103 us (0.963)
  the two profiles are of different devices: /device:TPU:15 before, /device:TPU:0 now
where the time goes in v1:
time: 103 us
  Pallas kernels  93.1 us (90%)
  local copies, waits for them, and re-layouts  7.92 us (8%)
    pallas_call x1, Pallas kernels, fused(): pl.pallas_call(functools.partial(layer_kernel, kv_size, tp_size), out_sha...  80.5 us
    pallas_call x1, Pallas kernels, update_state(): pl.pallas_call(state_kernel, grid=(seqs // group,), in_specs=[pl.BlockSpe...  12.6 us
    unnamed x3, local copies, waits for them, and re-layouts  2.54 us

profile of v1, /device:TPU:0, one launch (start us, length us, event | category | flops | bytes accessed | tf_op | source)
XLA Modules:
  0.0 102.5 jit_solution(17383842458594957350)
XLA Ops:
  0.6 0.8 and_convert_fusion.spread_ref
  1.5 2.5 %copy.27 = f32[128,4,512]{2,0,1:T(8,128)} copy(f32[128,4,512]{2,1,0:T(4,128)} %param.23) | data formatting | bytes 2097152 | tf_op args[10]
  4.0 1.7 %copy.22 = bf16[128,4,128]{2,0,1:T(8,128)(2,1)} copy(bf16[128,4,128]{0,2,1:T(8,128)(2,1)} %bitcast.19) | data formatting | bytes 262144 | tf_op jit(solution)/shard_map/reshape | solution.py:59
  5.7 1.4 %copy.23.acc_ref = s32[128,1]{1,0:T(8,128)} copy(s32[128,1]{0,1:T(1,128)} %bitcast.24) | data formatting | bytes 1024 | tf_op jit(solution)/shard_map/reshape | solution.py:86
  7.1 0.0 copy-start
  7.1 12.6 %shard_map.140 = (f32[128,4,32,128]{3,2,1,0:T(8,128)}, bf16[128,4,32,128]{3,2,1,0:T(8,128)(2,1)}) custom-call(s32[128,1]{1,0:T(8,128)} %copy.23.acc_ref, f32[4,128,512]{2,1,0:T(8,128)} %bitcast.17, bf16[4,128,128]{2,1,0:T(8,128)(2,1)} %bitcast.18, bf16[128,1024]{1,0:T(8,128)(2,1)} %and_convert_fusion.spread_ref, f32[128,4,32,128]{3,2,1,0:T(8,128)} %state_ref.1), custom_call_target="tpu_custom_call" | custom-call | flops 134217728 | bytes 20971520 | tf_op jit(solution)/shard_map/pallas_call | solution.py:64
  19.7 0.0 copy-done
  19.7 0.7 copy.20
  20.4 80.5 %shard_map.141 = bf16[512,128]{1,0:T(8,128)(2,1)} custom-call(bf16[512,128]{1,0:T(8,128)(2,1)} %bitcast.23, f32[1,4096]{1,0:T(1,128)} %bitcast.27, f32[1,512]{1,0:T(1,128)} %bitcast.28, f32[1,32]{1,0:T(1,128)} %bitcast.29, bf16[4096,512]{1,0:T(8,128)(2,1)} %wq_hbm.1, bf16[4096,512]{1,0:T(8,128)(2,1)} %wf_hbm.1, bf16[128,4096]{1,0:T(8,128)(2,1)} %bitcast.25, ...), custom_call_target="tpu_custom_call" | custom-call | flops 5905580032 | bytes 14680064 | tf_op jit(solution)/shard_map/pallas_call | solution.py:522
  100.9 1.7 %copy.28 = bf16[4,128,128]{2,0,1:T(4,128)(2,1)} copy(bf16[4,128,128]{2,1,0:T(8,128)(2,1)} %bitcast.22) | data formatting | bytes 262144 | tf_op jit(solution)/shard_map/reshape | solution.py:584
  (2 shorter events, 0.0 us)
Async XLA Ops:
  7.1 12.6 %copy-start = (bf16[128,4,128]{2,1,0:T(4,128)(2,1)S(1)}, bf16[128,4,128]{2,1,0:T(4,128)(2,1)}, u32[]{:S(2)}) copy-start(bf16[128,4,128]{2,1,0:T(4,128)(2,1)} %param.13) | copy-start | bytes 393220
